TPU v7x, 32 devices: a whole 2x2x4 slice. The times are simulated.
32 devices in a mesh: ep: 8 (over z, x), tp: 4 (over y, core).
Axes of the slice: x: 2, y: 2, z: 4, core: 2. Of those that a mesh axis runs over, the one named last changes fastest.
Arguments:
- tokens: bfloat16 [128, 4096], P('ep'), may hold values from -6 to 6
- norm_gain: float32 [4096], replicated, may hold values from 0.1 to 1.9
- query_weight: bfloat16 [4096, 2048], P('ep', 'tp'), may hold values from -0.09375 to 0.09375
- key_weight: bfloat16 [4096, 256], P('ep', 'tp'), may hold values from -0.09375 to 0.09375
- value_weight: bfloat16 [4096, 256], P('ep', 'tp'), may hold values from -0.09375 to 0.09375
- forget_weight: bfloat16 [4096, 32], P('ep', 'tp'), may hold values from -0.09375 to 0.09375
- forget_bias: float32 [32], P('tp'), may hold values from -1 to 2
- kv_cache: bfloat16 [128, 1024, 4, 128], P('ep', None, 'tp'), may hold values from -256 to 256, as said below
- log_gates: float32 [128, 1024, 32], P('ep', None, 'tp'), may hold values from -258 to 0
- lengths: int32 [128], P('ep'), may hold values from 128 to 1024, as said below
- out_weight: bfloat16 [2048, 4096], P('tp', 'ep'), may hold values from -0.125 to 0.125
- mix_gain: float32 [4096], replicated, may hold values from 0.1 to 1.9
- expert_gate: bfloat16 [8, 4096, 1024], P('ep', None, 'tp'), may hold values from -0.09375 to 0.09375
- expert_up: bfloat16 [8, 4096, 1024], P('ep', None, 'tp'), may hold values from -0.09375 to 0.09375
- expert_down: bfloat16 [8, 1024, 4096], P('ep', 'tp'), may hold values from -0.1875 to 0.1875
- routes: int32 [128, 4], P('ep'), may hold values from 0 to 7, all different within a row; in each aligned block of 16 rows (0 to 15, 16 to 31, ...) at most 16 rows name the same one
- route_weights: float32 [128, 4], P('ep'), may hold values from 0.2 to 1
- dense_gate: bfloat16 [4096, 4096], P(None, 'ep'), may hold values from -0.09375 to 0.09375
- dense_up: bfloat16 [4096, 4096], P(None, 'ep'), may hold values from -0.09375 to 0.09375
- dense_down: bfloat16 [4096, 4096], P('ep', 'tp'), may hold values from -0.09375 to 0.09375
- gate_vector: float32 [4096], replicated, may hold values from -0.09375 to 0.09375
Outputs:
- layer_out: bfloat16 [128, 4096], P('ep', 'tp')
Inputs may be any that keep to these rules, and one draw needn't show every extreme that they name: `kv_cache`: keys and values of the cached positions. `lengths`: some sequence uses all 1024 cached positions in every draw. A sequence's 4 experts differ. Among the routes of the 16 sequences of one index of ep no expert appears more than 16 times, and in every draw some expert appears exactly 16 times there; every expert is chosen somewhere.
All inputs are finite; a program needn't handle non-finite values.
Results may differ from a plain program's by a relative error of at most 0.012.
The roundings to bfloat16 on the way count: a program that leaves them out, or rounds other values in their place, can miss the bound.
Values may be sent and summed in bfloat16 or wider, within the bound.
A program may use at most 128 MiB of HBM per device.

v0:
```python
import jax
import jax.numpy as jnp
from jax import lax
from jax.sharding import PartitionSpec as P

EPS = 1e-06


def rms_scaled(matrix, gains):
    values = matrix.astype(jnp.float32)
    return values * lax.rsqrt(jnp.mean(values * values, axis=-1, keepdims=True) + EPS) * gains


def attend_local(queries, key_new, value_new, forget, kv_cache, log_gates, lengths):
    seqs_here, cache_len, kv_count, double_width = kv_cache.shape
    head_width = double_width // 2
    group_size = queries.shape[1] // (kv_count * head_width)
    queries = queries.reshape(seqs_here, kv_count, group_size, head_width)
    key_new = key_new.reshape(seqs_here, kv_count, head_width)
    value_new = value_new.reshape(seqs_here, kv_count, head_width)
    cached_keys = kv_cache[..., :head_width]
    cached_values = kv_cache[..., head_width:]
    score_scale = head_width ** (-0.5)
    current_position = jnp.arange(cache_len, dtype=jnp.int32)
    is_last = (current_position[None, :] == lengths[:, None] - 1)[:, :, None]
    last_gate = jnp.sum(jnp.where(is_last, log_gates, 0.0), axis=1)
    newest = last_gate + forget
    gate_bias = newest[:, None, :] - log_gates
    gate_bias = gate_bias.reshape(seqs_here, cache_len, kv_count, group_size).transpose(0, 2, 3, 1)
    past_scores = (
        jnp.einsum("skgd,slkd->skgl", queries, cached_keys, preferred_element_type=jnp.float32)
        * score_scale
        + gate_bias
    )
    is_valid = (current_position[None, :] < lengths[:, None])[:, None, None, :]
    past_scores = jnp.where(is_valid, past_scores, -jnp.inf)
    own_score = (
        jnp.einsum("skgd,skd->skg", queries, key_new, preferred_element_type=jnp.float32)
        * score_scale
    )
    highest = jnp.maximum(jnp.max(past_scores, axis=-1), own_score)
    past_exp = jnp.exp(past_scores - highest[..., None])
    own_exp = jnp.exp(own_score - highest)
    totals = jnp.sum(past_exp, axis=-1) + own_exp
    past_weights = (past_exp / totals[..., None]).astype(jnp.bfloat16)
    own_weights = (own_exp / totals).astype(jnp.bfloat16)
    mixed_values = jnp.einsum(
        "skgl,slkd->skgd", past_weights, cached_values, preferred_element_type=jnp.float32
    )
    mixed_values = (
        mixed_values
        + own_weights.astype(jnp.float32)[..., None] * value_new.astype(jnp.float32)[:, :, None, :]
    )
    return mixed_values.astype(jnp.bfloat16).reshape(seqs_here, kv_count * group_size * head_width)


def shards(
    tokens,
    norm_gain,
    query_weight,
    key_weight,
    value_weight,
    forget_weight,
    forget_bias,
    kv_cache,
    log_gates,
    lengths,
    out_weight,
    mix_gain,
    expert_gate,
    expert_up,
    expert_down,
    routes,
    route_weights,
    dense_gate,
    dense_up,
    dense_down,
    gate_vector,
):
    seq_count = tokens.shape[0]
    normed = rms_scaled(tokens, norm_gain).astype(jnp.bfloat16)
    query_cols = query_weight.shape[1]
    key_cols = key_weight.shape[1]
    columns = lax.all_to_all(normed, "ep", split_axis=1, concat_axis=0, tiled=True)
    row_block = columns
    projected = lax.psum_scatter(
        jnp.concatenate(
            [
                jnp.dot(row_block, matrix, preferred_element_type=jnp.float32)
                for matrix in (query_weight, key_weight, value_weight, forget_weight)
            ],
            axis=1,
        ),
        "ep",
        scatter_dimension=0,
        tiled=True,
    )
    queries = projected[:, :query_cols].astype(jnp.bfloat16)
    key_new = projected[:, query_cols : query_cols + key_cols].astype(jnp.bfloat16)
    value_new = projected[:, query_cols + key_cols : query_cols + 2 * key_cols].astype(jnp.bfloat16)
    forget = jax.nn.log_sigmoid(projected[:, query_cols + 2 * key_cols :] + forget_bias)
    attended = attend_local(queries, key_new, value_new, forget, kv_cache, log_gates, lengths)
    column_terms = jnp.dot(
        lax.all_gather(attended, "ep", axis=0, tiled=True),
        out_weight,
        preferred_element_type=jnp.float32,
    )
    column_total = lax.psum(column_terms, "tp")
    summed = lax.all_to_all(column_total, "ep", split_axis=0, concat_axis=1, tiled=True)
    mixed = (tokens.astype(jnp.float32) + summed).astype(jnp.bfloat16)
    second = rms_scaled(mixed, mix_gain).astype(jnp.bfloat16)
    gate_value = jax.nn.sigmoid(
        jnp.dot(second.astype(jnp.float32), gate_vector, precision=lax.Precision.HIGHEST)
    )
    experts = lax.axis_size("ep")
    top_count = routes.shape[1]
    capacity = max(2, 2 * seq_count * top_count // experts)
    flat_routes = routes.reshape(-1)
    one_hot = (flat_routes[:, None] == jnp.arange(experts, dtype=jnp.int32)[None, :]).astype(
        jnp.int32
    )
    earlier = jnp.sum((jnp.cumsum(one_hot, axis=0) - one_hot) * one_hot, axis=1)
    slot_index = (flat_routes * capacity + earlier).reshape(seq_count, top_count)
    slot_ids = jnp.arange(experts * capacity, dtype=jnp.int32)
    dispatch_map = jnp.any(slot_index[None, :, :] == slot_ids[:, None, None], axis=2).astype(
        jnp.bfloat16
    )
    outgoing = jnp.dot(dispatch_map, second, preferred_element_type=jnp.float32).astype(
        jnp.bfloat16
    )
    outgoing = outgoing.reshape(experts, capacity, second.shape[1])
    received = lax.all_to_all(outgoing, "ep", split_axis=0, concat_axis=0, tiled=True)
    sources, items, model_width = received.shape
    flat_rows = received.reshape(sources * items, model_width)
    gate_pre = jnp.dot(flat_rows, expert_gate[0], preferred_element_type=jnp.float32)
    up_pre = jnp.dot(flat_rows, expert_up[0], preferred_element_type=jnp.float32)
    hidden = (jax.nn.silu(gate_pre) * up_pre).astype(jnp.bfloat16)
    partial_rows = jnp.dot(hidden, expert_down[0], preferred_element_type=jnp.float32)
    reduced = lax.psum_scatter(partial_rows, "tp", scatter_dimension=1, tiled=True)
    replies = reduced.astype(jnp.bfloat16).reshape(sources, items, reduced.shape[1])
    returned = lax.all_to_all(replies, "ep", split_axis=0, concat_axis=0, tiled=True)
    quarter_cols = returned.shape[2]
    picked = returned.reshape(experts * capacity, quarter_cols)[slot_index.reshape(-1)]
    routed = jnp.sum(
        picked.astype(jnp.float32).reshape(seq_count, top_count, quarter_cols)
        * route_weights[:, :, None],
        axis=1,
    )
    tp_index = lax.axis_index("tp")
    piece = lax.all_gather(second, "ep", axis=0, tiled=True)
    dense_hidden = (
        jax.nn.silu(jnp.dot(piece, dense_gate, preferred_element_type=jnp.float32))
        * jnp.dot(piece, dense_up, preferred_element_type=jnp.float32)
    ).astype(jnp.bfloat16)
    row_block = dense_hidden
    dense_out = lax.psum_scatter(
        jnp.dot(row_block, dense_down, preferred_element_type=jnp.float32),
        "ep",
        scatter_dimension=0,
        tiled=True,
    )
    residual = lax.dynamic_slice_in_dim(mixed, tp_index * quarter_cols, quarter_cols, 1).astype(
        jnp.float32
    )
    return (residual + routed + gate_value[:, None] * dense_out).astype(jnp.bfloat16)


def solution(mesh):
    return jax.shard_map(
        shards,
        mesh=mesh,
        in_specs=(
            P("ep", None),
            P(),
            P("ep", "tp"),
            P("ep", "tp"),
            P("ep", "tp"),
            P("ep", "tp"),
            P("tp"),
            P("ep", None, "tp", None),
            P("ep", None, "tp"),
            P("ep"),
            P("tp", "ep"),
            P(),
            P("ep", None, "tp"),
            P("ep", None, "tp"),
            P("ep", "tp", None),
            P("ep", None),
            P("ep", None),
            P(None, "ep"),
            P(None, "ep"),
            P("ep", "tp"),
            P(),
        ),
        out_specs=P("ep", "tp"),
        check_vma=False,
    )
```

profile of v0, /device:TPU:0, one launch (start us, length us, event | category | flops | bytes accessed | tf_op | source)
XLA Modules:
  0.0 333.0 jit_solution(12179301577359732236)
XLA Ops:
  6.6 1.2 fusion.48
  7.8 1.0 fusion.50
  8.9 14.4 %all_to_all.48 = bf16[16,8,512]{2,0,1:T(8,128)(2,1)S(1)} all-to-all(bf16[16,8,512]{2,0,1:T(8,128)(2,1)S(1)} %bitcast.121), channel_id=1, replica_groups=mesh['ep'=8,'tp'=4] {'ep'}, dimensions={1} | all-to-all | bytes 262144 | tf_op jit(solution)/shard_map/all_to_all | solution.py:84
  23.3 0.8 fusion.84
  24.1 1.0 fusion.83
  25.2 1.0 fusion.82
  26.2 1.3 fusion.81
  27.5 0.9 pad_maximum_fusion
  28.4 0.7 broadcast_add_fusion
  29.1 0.2 select_reduce_fusion
  29.4 59.1 %reduce-scatter.4.cloned.1.call-done = f32[16,648]{1,0:T(8,128)} async-done(((f32[128,648]{1,0:T(8,128)}), f32[16,648]{1,0:T(8,128)}) %reduce-scatter.4.cloned.1.call-update) | async-done | bytes 41488 | tf_op jit(solution)/shard_map/reduce_scatter | solution.py:86
  88.5 0.8 convert.6
  89.4 0.1 reshape.186
  89.5 0.1 fusion.71
  89.6 0.9 fusion.69
  90.5 3.7 %fusion.80 = (f32[16,8]{1,0:T(8,128)S(1)}, f32[16,1,8,1024]{3,2,0,1:T(8,128)S(1)}) fusion(f32[16,1024,8]{1,2,0:T(8,128)S(1)} %copy-done.3, f32[16,8]{1,0:T(8,128)S(1)} %fusion.69, bf16[16,8,64]{2,1,0:T(8,128)(2,1)S(1)} %reshape.186, bf16[16,1024,1,128]{3,1,2,0:T(8,128)(2,1)} %param.28, pred[16,1024]{1,0:T(8,128)(4,1)S(1)} %iota_compare_fusion.1), kind=kOutput, calls=%fused_computation.96 | convolution fusion | flops 17432448 | bytes 5276672 | tf_op jit(solution)/shard_map/skgd,slkd->skgl/dot_general | solution.py:31
  94.2 0.2 fusion.44
  94.5 1.4 fusion.37
  95.9 0.1 reshape.191
  96.0 30.5 %all_gather.6 = bf16[128,512]{1,0:T(8,128)(2,1)S(1)} all-gather(bf16[16,512]{1,0:T(8,128)(2,1)S(1)} %reshape.191), channel_id=1, replica_groups=mesh['ep'=8,'tp'=4] {'ep'}, dimensions={0}, use_global_device_ids=true | all-gather | bytes 147456 | tf_op jit(solution)/shard_map/all_gather | solution.py:104
  126.6 0.9 fusion.85
  127.7 31.3 %all-reduce.2.cloned.1.call-done = f32[8,16,512]{2,1,0:T(8,128)} async-done(((f32[8,16,512]{2,1,0:T(8,128)}), f32[8,16,512]{2,1,0:T(8,128)}) %all-reduce.2.cloned.1.call-update) | async-done | bytes 262160 | tf_op jit(solution)/shard_map/psum | solution.py:108
  159.0 5.5 %all-to-all-start.1 = ((f32[8,16,512]{2,1,0:T(8,128)}), f32[8,16,512]{2,1,0:T(8,128)S(1)}, u32[]{:S(2)}, u32[]{:S(2)}) async-start(f32[8,16,512]{2,1,0:T(8,128)} %all-reduce.2.cloned.1.call-done), calls=%async_computation.2 | async-start | bytes 524288 | tf_op jit(solution)/shard_map/all_to_all | solution.py:109
  164.6 0.1 reduce_window_sum.11
  164.7 0.2 select_reduce_fusion.1
  165.1 0.1 fusion.67
  165.2 7.6 %all-to-all-done.1 = f32[8,16,512]{2,1,0:T(8,128)S(1)} async-done(((f32[8,16,512]{2,1,0:T(8,128)}), f32[8,16,512]{2,1,0:T(8,128)S(1)}, u32[]{:S(2)}, u32[]{:S(2)}) %all-to-all-start.1) | async-done | bytes 262176 | tf_op jit(solution)/shard_map/all_to_all | solution.py:109
  172.8 0.2 fusion.45
  173.0 0.1 fusion.47
  173.1 1.5 convolution_convert_fusion
  174.6 3.6 %all-to-all-start.2 = ((bf16[8,16,4096]{2,1,0:T(8,128)(2,1)}), bf16[8,16,4096]{2,1,0:T(8,128)(2,1)S(1)}, u32[]{:S(2)}, u32[]{:S(2)}) async-start(bf16[8,16,4096]{2,1,0:T(8,128)(2,1)} %bitcast.112), calls=%async_computation.3 | async-start | bytes 2097152 | tf_op jit(solution)/shard_map/all_to_all | solution.py:132
  178.2 0.7 all-gather.2.cloned.1.call-update
  178.9 27.4 %all-to-all-done.2 = bf16[8,16,4096]{2,1,0:T(8,128)(2,1)S(1)} async-done(((bf16[8,16,4096]{2,1,0:T(8,128)(2,1)}), bf16[8,16,4096]{2,1,0:T(8,128)(2,1)S(1)}, u32[]{:S(2)}, u32[]{:S(2)}) %all-to-all-start.2) | async-done | bytes 1048608 | tf_op jit(solution)/shard_map/all_to_all | solution.py:132
  206.3 2.0 fusion.10
  208.4 4.3 %fusion.6 = f32[128,4096]{1,0:T(8,128)} fusion(bf16[1,256,4096]{2,1,0:T(8,128)(2,1)S(1)} %copy-done, bf16[128,4096]{1,0:T(8,128)(2,1)S(1)} %bitcast.110, bf16[1,4096,256]{2,1,0:T(8,128)(2,1)} %param.34, f32[128,256]{1,0:T(8,128)S(1)} %fusion.10), kind=kOutput, calls=%fused_computation.8 | convolution fusion | flops 537067520 | bytes 7471104 | tf_op jit(solution)/shard_map/dot_general | solution.py:138
  212.7 14.0 %all-gather.2.cloned.1.call-done = bf16[128,4096]{1,0:T(8,128)(2,1)} async-done(((bf16[16,4096]{1,0:T(8,128)(2,1)}), bf16[128,4096]{1,0:T(8,128)(2,1)}) %all-gather.2.cloned.1.call-update) | async-done | bytes 1048592 | tf_op jit(solution)/shard_map/all_gather | solution.py:150
  226.7 3.3 fusion.86
  230.1 4.3 %fusion.25 = f32[128,1024]{1,0:T(8,128)} fusion(bf16[512,1024]{1,0:T(8,128)(2,1)} %param.40, bf16[128,4096]{1,0:T(8,128)(2,1)S(1)} %copy-done.2, bf16[4096,512]{1,0:T(8,128)(2,1)} %param.39, f32[128,512]{1,0:T(8,128)S(1)} %fusion.86), kind=kOutput, calls=%fused_computation.20 | convolution fusion | flops 671481856 | bytes 7077888 | tf_op jit(solution)/shard_map/dot_general | solution.py:157
  234.6 24.5 %reduce-scatter.6.cloned.1.call-done = f32[128,1024]{1,0:T(8,128)} async-done(((f32[128,4096]{1,0:T(8,128)}), f32[128,1024]{1,0:T(8,128)}) %reduce-scatter.6.cloned.1.call-update) | async-done | bytes 524304 | tf_op jit(solution)/shard_map/reduce_scatter | solution.py:139
  259.0 1.8 convert_element_type.82
  260.8 5.5 %all-to-all-start.3 = ((bf16[8,16,1024]{2,1,0:T(8,128)(2,1)}), bf16[8,16,1024]{2,1,0:T(8,128)(2,1)S(1)}, u32[]{:S(2)}, u32[]{:S(2)}) async-start(bf16[8,16,1024]{2,1,0:T(8,128)(2,1)} %bitcast.19), calls=%async_computation.5 | async-start | bytes 524288 | tf_op jit(solution)/shard_map/all_to_all | solution.py:141
  266.4 0.9 fusion.43
  267.3 8.6 %all-to-all-done.3 = bf16[8,16,1024]{2,1,0:T(8,128)(2,1)S(1)} async-done(((bf16[8,16,1024]{2,1,0:T(8,128)(2,1)}), bf16[8,16,1024]{2,1,0:T(8,128)(2,1)S(1)}, u32[]{:S(2)}, u32[]{:S(2)}) %all-to-all-start.3) | async-done | bytes 262176 | tf_op jit(solution)/shard_map/all_to_all | solution.py:141
  275.9 0.7 gather_fusion
  276.6 0.1 reshape.196
  276.7 0.2 multiply_reduce_fusion
  276.9 48.0 %reduce-scatter.8.cloned.1.call-done = f32[16,1024]{1,0:T(8,128)} async-done(((f32[128,1024]{1,0:T(8,128)}), f32[16,1024]{1,0:T(8,128)}) %reduce-scatter.8.cloned.1.call-update) | async-done | bytes 65552 | tf_op jit(solution)/shard_map/reduce_scatter | solution.py:156
  324.9 1.5 add_convert_fusion
  (57 shorter events, 1.2 us)
Async XLA Ops:
  6.5 201.8 %copy-start = (bf16[1,256,4096]{2,1,0:T(8,128)(2,1)S(1)}, bf16[1,256,4096]{2,1,0:T(8,128)(2,1)}, u32[]{:S(2)}) copy-start(bf16[1,256,4096]{2,1,0:T(8,128)(2,1)} %param.35) | copy-start | bytes 6291460
  6.5 22.8 %copy-start.12 = (s32[16]{0:T(128)S(1)}, s32[16]{0:T(128)}, u32[]{:S(2)}) copy-start(s32[16]{0:T(128)} %param.30) | copy-start | bytes 196
  6.5 22.6 %copy-start.3 = (f32[16,1024,8]{1,2,0:T(8,128)S(1)}, f32[16,1024,8]{1,2,0:T(8,128)}, u32[]{:S(2)}) copy-start(f32[16,1024,8]{1,2,0:T(8,128)} %param.29) | copy-start | bytes 1572868
  6.5 83.1 %copy-start.13 = (f32[8]{0:T(128)S(1)}, f32[8]{0:T(128)}, u32[]{:S(2)}) copy-start(f32[8]{0:T(128)} %param.27) | copy-start | bytes 100
  6.5 82.0 %reduce-scatter.4.cloned.1.call-start = ((), (), s32[]{:S(2)}) async-start(), calls=%async_computation.7 | async-start | bytes 442368 | tf_op jit(solution)/shard_map/reduce_scatter | solution.py:86
  28.3 130.7 %all-reduce.2.cloned.1.call-start = ((), (), s32[]{:S(2)}) async-start(), calls=%async_computation.8 | async-start | bytes 524288 | tf_op jit(solution)/shard_map/psum | solution.py:108
  89.5 5.0 %copy-start.1 = (bf16[16,1024,1,128]{3,1,2,0:T(8,128)(2,1)S(1)}, bf16[16,1024,1,128]{3,1,2,0:T(8,128)(2,1)}, u32[]{:S(2)}) copy-start(bf16[16,1024,1,128]{3,1,2,0:T(8,128)(2,1)} %param.28) | copy-start | bytes 12582916
  94.2 32.3 %copy-start.8 = (bf16[512,512]{1,0:T(8,128)(2,1)S(1)}, bf16[512,512]{1,0:T(8,128)(2,1)}, u32[]{:S(2)}) copy-start(bf16[512,512]{1,0:T(8,128)(2,1)} %param.31) | copy-start | bytes 1572868
  94.2 33.3 %copy-start.10 = (s32[16,4]{0,1:T(4,128)S(1)}, s32[16,4]{0,1:T(4,128)}, u32[]{:S(2)}) copy-start(s32[16,4]{0,1:T(4,128)} %param.36) | copy-start | bytes 772
  94.5 78.3 %copy-start.4 = (bf16[16,4096]{1,0:T(8,128)(2,1)S(1)}, bf16[16,4096]{1,0:T(8,128)(2,1)}, u32[]{:S(2)}) copy-start(bf16[16,4096]{1,0:T(8,128)(2,1)} %param.21) | copy-start | bytes 393220
  94.5 78.5 %copy-start.9 = (f32[4096]{0:T(1024)S(1)}, f32[4096]{0:T(1024)}, u32[]{:S(2)}) copy-start(f32[4096]{0:T(1024)} %param.32) | copy-start | bytes 49156
  159.0 13.7 %all-to-all-start.1 = ((f32[8,16,512]{2,1,0:T(8,128)}), f32[8,16,512]{2,1,0:T(8,128)S(1)}, u32[]{:S(2)}, u32[]{:S(2)}) async-start(f32[8,16,512]{2,1,0:T(8,128)} %all-reduce.2.cloned.1.call-done), calls=%async_computation.2 | async-start | bytes 524288 | tf_op jit(solution)/shard_map/all_to_all | solution.py:109
  173.0 1.6 copy-start.7
  173.1 5.1 %copy-start.5 = (bf16[16,4096]{1,0:T(8,128)(2,1)}, bf16[16,4096]{1,0:T(8,128)(2,1)S(1)}, u32[]{:S(2)}) copy-start(bf16[16,4096]{1,0:T(8,128)(2,1)S(1)} %fusion.47) | copy-start | bytes 393220
  174.6 31.8 %all-to-all-start.2 = ((bf16[8,16,4096]{2,1,0:T(8,128)(2,1)}), bf16[8,16,4096]{2,1,0:T(8,128)(2,1)S(1)}, u32[]{:S(2)}, u32[]{:S(2)}) async-start(bf16[8,16,4096]{2,1,0:T(8,128)(2,1)} %bitcast.112), calls=%async_computation.3 | async-start | bytes 2097152 | tf_op jit(solution)/shard_map/all_to_all | solution.py:132
  178.1 48.6 %all-gather.2.cloned.1.call-start = ((), (), s32[]{:S(2)}) async-start(), calls=%async_computation.10 | async-start | bytes 1179648 | tf_op jit(solution)/shard_map/all_gather | solution.py:150
  178.9 80.2 %reduce-scatter.6.cloned.1.call-start = ((), (), s32[]{:S(2)}) async-start(), calls=%async_computation.9 | async-start | bytes 2621440 | tf_op jit(solution)/shard_map/reduce_scatter | solution.py:139
  212.7 112.2 %reduce-scatter.8.cloned.1.call-start = ((), (), s32[]{:S(2)}) async-start(), calls=%async_computation.11 | async-start | bytes 589824 | tf_op jit(solution)/shard_map/reduce_scatter | solution.py:156
  226.7 3.3 copy-start.2
  230.1 4.3 %copy-start.11 = (f32[16,4]{0,1:T(4,128)S(1)}, f32[16,4]{0,1:T(4,128)}, u32[]{:S(2)}) copy-start(f32[16,4]{0,1:T(4,128)} %param.37) | copy-start | bytes 772
  230.1 36.3 %copy-start.6 = (bf16[16,4096]{1,0:T(8,128)(2,1)S(1)}, bf16[16,4096]{1,0:T(8,128)(2,1)}, u32[]{:S(2)}) copy-start(bf16[16,4096]{1,0:T(8,128)(2,1)} %copy-done.5) | copy-start | bytes 393220
  260.8 15.1 %all-to-all-start.3 = ((bf16[8,16,1024]{2,1,0:T(8,128)(2,1)}), bf16[8,16,1024]{2,1,0:T(8,128)(2,1)S(1)}, u32[]{:S(2)}, u32[]{:S(2)}) async-start(bf16[8,16,1024]{2,1,0:T(8,128)(2,1)} %bitcast.19), calls=%async_computation.5 | async-start | bytes 524288 | tf_op jit(solution)/shard_map/all_to_all | solution.py:141
Sparse Core Ops, SparseCore 0:
  28.5 60.0 reduce-scatter.3
  127.6 31.3 all-reduce.1
  181.1 45.6 all-gather.1
  229.1 29.8 reduce-scatter.5
  262.2 62.6 reduce-scatter.7
where the time goes:
time: 334 us; the launch traced here: 333 us
  waiting for transfers between devices  221 us (66%)
  blocking collectives  44.9 us (13%)
  matrix products  26.6 us (8%)
  starting transfers between devices  14.8 us (4%)
  between operations  13.5 us (4%)
  other arithmetic  10.4 us (3%)
    reduce_scatter x1, waiting for transfers between devices, shards(): lax.psum_scatter(jnp.concatenate([jnp.dot(row_block, matrix, preferred_el...  59.1 us
    reduce_scatter x1, waiting for transfers between devices, shards(): lax.psum_scatter(jnp.dot(row_block, dense_down, preferred_element_type=jn...  48 us
    psum x1, waiting for transfers between devices, shards(): column_total = lax.psum(column_terms, 'tp')  31.3 us
    all_gather x1, blocking collectives, shards(): lax.all_gather(attended, 'ep', axis=0, tiled=True)  30.5 us
    all_to_all x1, waiting for transfers between devices, shards(): lax.all_to_all(outgoing, 'ep', split_axis=0, concat_axis=0, tiled=True)  27.4 us
    reduce_scatter x1, waiting for transfers between devices, shards(): lax.psum_scatter(partial_rows, 'tp', scatter_dimension=1, tiled=True)  24.5 us
    all_to_all x1, blocking collectives, shards(): lax.all_to_all(normed, 'ep', split_axis=1, concat_axis=0, tiled=True)  14.4 us
    all_gather x1, waiting for transfers between devices, shards(): piece = lax.all_gather(second, 'ep', axis=0, tiled=True)  14 us
  transfers between devices with their start and end apart: 8, of which 8 were waited for; matrix products, arithmetic and copies ran while one was open for 6% of the time, Pallas kernels for 0%

commit v1 on v0

--- a/solution.py
+++ b/solution.py
@@ -1,6 +1,10 @@
+import functools
+
 import jax
 import jax.numpy as jnp
 from jax import lax
+from jax.experimental import pallas as pl
+from jax.experimental.pallas import tpu as pltpu
 from jax.sharding import PartitionSpec as P
 
 EPS = 1e-06
@@ -165,9 +169,446 @@
     return (residual + routed + gate_value[:, None] * dense_out).astype(jnp.bfloat16)
 
 
+MESH = pl.DeviceIdType.MESH
+LANES = 128
+
+
+def nt_dot(a, b):
+    return lax.dot_general(a, b, (((1,), (1,)), ((), ())), preferred_element_type=jnp.float32)
+
+
+def remote(src, dst, send_sem, recv_sem, ep, tp):
+    copy = pltpu.make_async_remote_copy(
+        src_ref=src,
+        dst_ref=dst,
+        send_sem=send_sem,
+        recv_sem=recv_sem,
+        device_id=(ep, tp),
+        device_id_type=MESH,
+    )
+    copy.start()
+    return copy
+
+
+def front_kernel(
+    n_ep,
+    tok_ref,
+    gain_ref,
+    wmat_ref,
+    wq_ref,
+    wk_ref,
+    wv_ref,
+    wf_ref,
+    proj_ref,
+    tokc_ref,
+    aux_ref,
+    aux_own,
+    part,
+    part_in,
+    ts_sem,
+    tr_sem,
+    as_sem,
+    ar_sem,
+    ps_sem,
+    pr_sem,
+):
+    e = lax.axis_index("ep")
+    t = lax.axis_index("tp")
+    seqs, width = tok_ref.shape
+    cols = width // n_ep
+    barrier = pltpu.get_barrier_semaphore()
+    for o in range(1, n_ep):
+        pl.semaphore_signal(
+            barrier, inc=1, device_id=(lax.rem(e + o, n_ep), t), device_id_type=MESH
+        )
+    tokens = tok_ref[...].astype(jnp.float32)
+    scale = lax.rsqrt(jnp.mean(tokens * tokens, axis=-1, keepdims=True) + EPS)
+    lane = lax.broadcasted_iota(jnp.int32, (seqs, LANES), 1)
+    aux_own[...] = jnp.where(lane == LANES - 1, scale, wmat_ref[...])
+    pl.semaphore_wait(barrier, n_ep - 1)
+    copies = []
+    for o in range(1, n_ep):
+        peer = lax.rem(e + o, n_ep)
+        chunk = pl.ds(pl.multiple_of(peer * cols, LANES), cols)
+        copies.append(
+            remote(tok_ref.at[:, chunk], tokc_ref.at[e], ts_sem.at[o], tr_sem.at[o], peer, t)
+        )
+        copies.append(remote(aux_own, aux_ref.at[e], as_sem.at[o], ar_sem.at[o], peer, t))
+    tokc_ref[e] = tok_ref[:, pl.ds(pl.multiple_of(e * cols, LANES), cols)]
+    aux_ref[e] = aux_own[...]
+    for copy in copies:
+        copy.wait_recv()
+    rows = n_ep * seqs
+    scales = aux_ref[...].reshape(rows, LANES)[:, LANES - 1 :]
+    block = tokc_ref[...].reshape(rows, cols).astype(jnp.float32)
+    normed = (block * scales * gain_ref[pl.ds(e, 1), :]).astype(jnp.bfloat16)
+    queries = jnp.dot(normed, wq_ref[...], preferred_element_type=jnp.float32)
+    qc = queries.shape[1]
+    kc = wk_ref.shape[0]
+    fc = wf_ref.shape[0]
+    part[:, :, :qc] = queries.reshape(n_ep, seqs, qc)
+    rest = [nt_dot(normed, wk_ref[...]), nt_dot(normed, wv_ref[...]), nt_dot(normed, wf_ref[...])]
+    fill = part.shape[2] - qc - 2 * kc - fc
+    rest = jnp.concatenate(rest + [jnp.zeros((rows, fill), jnp.float32)], axis=1)
+    part[:, :, qc:] = rest.reshape(n_ep, seqs, rest.shape[1])
+    sums = []
+    for o in range(1, n_ep):
+        peer = lax.rem(e + o, n_ep)
+        sums.append(remote(part.at[peer], part_in.at[o], ps_sem.at[o], pr_sem.at[o], peer, t))
+    total = part[e]
+    for o in range(1, n_ep):
+        sums[o - 1].wait_recv()
+        total = total + part_in[o]
+    proj_ref[...] = total
+    for copy in copies + sums:
+        copy.wait_send()
+
+
+def back_kernel(
+    n_ep,
+    n_tp,
+    att_ref,
+    tokc_ref,
+    aux_ref,
+    gain_ref,
+    vector_ref,
+    ow_hbm,
+    eg_hbm,
+    eu_hbm,
+    ed_hbm,
+    dg_hbm,
+    du_hbm,
+    dd_hbm,
+    out_ref,
+    ow,
+    eg,
+    eu,
+    ed,
+    dg,
+    du,
+    dd,
+    att,
+    osend,
+    orecv,
+    mix,
+    sec,
+    dsend,
+    drecv,
+    ysend,
+    yrecv,
+    csend,
+    crecv,
+    w_sem,
+    a_sem,
+    o_sem,
+    g_sem,
+    gy_sem,
+    gd_sem,
+    d_sem,
+    y_sem,
+    c_sem,
+):
+    e = lax.axis_index("ep")
+    t = lax.axis_index("tp")
+    ty = lax.rem(t + 2, n_tp)
+    td = t + 1 - 2 * lax.rem(t, 2)
+    tdy = lax.rem(td + 2, n_tp)
+    seqs = att_ref.shape[0]
+    rows = n_ep * seqs
+    loads = [
+        pltpu.make_async_copy(src, dst, w_sem.at[i])
+        for i, (src, dst) in enumerate(
+            [
+                (ow_hbm, ow),
+                (eg_hbm.at[0], eg),
+                (eu_hbm.at[0], eu),
+                (ed_hbm.at[0], ed),
+                (dg_hbm, dg),
+                (du_hbm, du),
+                (dd_hbm, dd),
+            ]
+        )
+    ]
+    for load in loads:
+        load.start()
+    barrier = pltpu.get_barrier_semaphore()
+    for o in range(1, n_ep):
+        pl.semaphore_signal(
+            barrier, inc=1, device_id=(lax.rem(e + o, n_ep), t), device_id_type=MESH
+        )
+    for o in range(1, n_tp):
+        pl.semaphore_signal(
+            barrier, inc=1, device_id=(e, lax.rem(t + o, n_tp)), device_id_type=MESH
+        )
+    pl.semaphore_wait(barrier, n_ep + n_tp - 2)
+    pending = []
+    copies = []
+    for o in range(1, n_ep):
+        peer = lax.rem(e + o, n_ep)
+        copies.append(remote(att_ref, att.at[e], a_sem.at[0, o], a_sem.at[1, o], peer, t))
+    att[e] = att_ref[...]
+    loads[0].wait()
+    for copy in copies:
+        copy.wait_recv()
+    pending += copies
+    partial = jnp.dot(
+        att[...].reshape(rows, att_ref.shape[1]), ow[...], preferred_element_type=jnp.float32
+    )
+    cw = osend.shape[2]
+    for j in range(n_tp):
+        osend[j] = partial[:, j * cw : (j + 1) * cw]
+    copies = []
+    for o in range(1, n_tp):
+        peer = lax.rem(t + o, n_tp)
+        copies.append(
+            remote(osend.at[peer], orecv.at[o], o_sem.at[0, o], o_sem.at[1, o], e, peer)
+        )
+    total = osend[t]
+    for o in range(1, n_tp):
+        copies[o - 1].wait_recv()
+        total = total + orecv[o]
+    pending += copies
+    own_tokens = tokc_ref[:, :, pl.ds(pl.multiple_of(t * cw, LANES), cw)].reshape(rows, cw)
+    mix[t, e] = (own_tokens.astype(jnp.float32) + total).astype(jnp.bfloat16)
+    arrivals, y_copies, d_copies = [], [], []
+    for o in range(1, n_ep):
+        peer = lax.rem(e + o, n_ep)
+        arrivals.append(
+            remote(mix.at[t, e], mix.at[t, e], g_sem.at[0, o], g_sem.at[1, o], peer, t)
+        )
+    for o in range(n_ep + 1):
+        if o < n_ep:
+            slot = mix.at[t, lax.rem(e + n_ep - o, n_ep)]
+            if o > 0:
+                arrivals[o - 1].wait_recv()
+            y_copies.append(remote(slot, slot, gy_sem.at[0, o], gy_sem.at[1, o], e, ty))
+            d_copies.append(remote(slot, slot, gd_sem.at[0, 0, o], gd_sem.at[1, 0, o], e, td))
+        if o > 0:
+            slot = mix.at[ty, lax.rem(e + n_ep - (o - 1), n_ep)]
+            y_copies[o - 1].wait_recv()
+            d_copies.append(
+                remote(slot, slot, gd_sem.at[0, 1, o - 1], gd_sem.at[1, 1, o - 1], e, td)
+            )
+    for copy in d_copies:
+        copy.wait_recv()
+    pending += arrivals + y_copies + d_copies
+    squares = jnp.zeros((rows, cw), jnp.float32)
+    for j in range(n_tp):
+        for i in range(n_ep):
+            values = mix[j, i].astype(jnp.float32)
+            squares = squares + values * values
+    scale = lax.rsqrt(jnp.sum(squares, axis=-1, keepdims=True) / sec.shape[1] + EPS)
+    gates = jnp.zeros((rows, cw), jnp.float32)
+    for i in range(n_ep):
+        for j in range(n_tp):
+            at = (i * n_tp + j) * cw
+            values = mix[j, i].astype(jnp.float32) * scale * gain_ref[:, at : at + cw]
+            values = values.astype(jnp.bfloat16)
+            sec[:, at : at + cw] = values
+            gates = gates + values.astype(jnp.float32) * vector_ref[:, at : at + cw]
+    gate_value = jax.nn.sigmoid(jnp.sum(gates, axis=-1, keepdims=True))
+    for load in loads[1:4]:
+        load.wait()
+    hidden = (
+        jax.nn.silu(jnp.dot(sec[...], eg[...], preferred_element_type=jnp.float32))
+        * jnp.dot(sec[...], eu[...], preferred_element_type=jnp.float32)
+    ).astype(jnp.bfloat16)
+    ocols = out_ref.shape[1]
+
+    def down(owner):
+        chunk = pl.ds(pl.multiple_of(owner * ocols, LANES), ocols)
+        return jnp.dot(hidden, ed[:, chunk], preferred_element_type=jnp.float32)
+
+    pair = []
+    for k, owner in enumerate((tdy, td)):
+        dsend[k] = down(owner)
+        pair.append(
+            remote(dsend.at[k], drecv.at[k], d_sem.at[0, k], d_sem.at[1, k], e, td)
+        )
+    across = down(ty)
+    pair[0].wait_recv()
+    ysend[...] = (across + drecv[0]).astype(jnp.bfloat16)
+    y_copy = remote(ysend, yrecv, y_sem.at[0], y_sem.at[1], e, ty)
+    own = down(t)
+    for load in loads[4:]:
+        load.wait()
+    dense_hidden = (
+        jax.nn.silu(jnp.dot(sec[...], dg[...], preferred_element_type=jnp.float32))
+        * jnp.dot(sec[...], du[...], preferred_element_type=jnp.float32)
+    ).astype(jnp.bfloat16)
+    dense = jnp.dot(dense_hidden, dd[...], preferred_element_type=jnp.float32)
+    pair[1].wait_recv()
+    y_copy.wait_recv()
+    expert_out = (own + drecv[1] + yrecv[...].astype(jnp.float32)).astype(jnp.bfloat16)
+    pending += pair + [y_copy]
+    aux = aux_ref[...].reshape(rows, LANES)
+    lane = lax.broadcasted_iota(jnp.int32, (rows, LANES), 1)
+    weight = jnp.sum(jnp.where(lane == e, aux, 0.0), axis=-1, keepdims=True)
+    terms = weight * expert_out.astype(jnp.float32) + gate_value * dense
+    csend[...] = terms.astype(jnp.bfloat16).reshape(n_ep, seqs, ocols)
+    copies = []
+    for o in range(1, n_ep):
+        peer = lax.rem(e + o, n_ep)
+        copies.append(
+            remote(csend.at[peer], crecv.at[o], c_sem.at[0, o], c_sem.at[1, o], peer, t)
+        )
+    mine = pl.ds(pl.multiple_of(e * seqs, seqs), seqs)
+    per_tp = n_ep // n_tp
+    pieces = [mix[j, t * per_tp + k, mine, :] for k in range(per_tp) for j in range(n_tp)]
+    total = jnp.concatenate(pieces, axis=1).astype(jnp.float32)
+    total = total + csend[e].astype(jnp.float32)
+    for o in range(1, n_ep):
+        copies[o - 1].wait_recv()
+        total = total + crecv[o].astype(jnp.float32)
+    out_ref[...] = total.astype(jnp.bfloat16)
+    for copy in pending + copies:
+        copy.wait_send()
+
+
+def fused_shards(
+    tokens,
+    norm_gain,
+    query_weight,
+    key_weight,
+    value_weight,
+    forget_weight,
+    forget_bias,
+    kv_cache,
+    log_gates,
+    lengths,
+    out_weight,
+    mix_gain,
+    expert_gate,
+    expert_up,
+    expert_down,
+    routes,
+    route_weights,
+    dense_gate,
+    dense_up,
+    dense_down,
+    gate_vector,
+):
+    n_ep = lax.axis_size("ep")
+    n_tp = lax.axis_size("tp")
+    seqs, width = tokens.shape
+    rows = n_ep * seqs
+    cols = width // n_ep
+    qc = query_weight.shape[1]
+    kc = key_weight.shape[1]
+    fc = forget_weight.shape[1]
+    pw = qc + -(-(2 * kc + fc) // LANES) * LANES
+    vmem = pl.BlockSpec(memory_space=pltpu.VMEM)
+    anywhere = pl.BlockSpec(memory_space=pl.ANY)
+    dma = pltpu.SemaphoreType.DMA
+    f32, bf16 = jnp.float32, jnp.bfloat16
+    chosen = routes[:, :, None] == jnp.arange(LANES, dtype=jnp.int32)[None, None, :]
+    wmat = jnp.sum(jnp.where(chosen, route_weights[:, :, None], 0.0), axis=1)
+    projected, token_cols, aux = pl.pallas_call(
+        functools.partial(front_kernel, n_ep),
+        out_shape=(
+            jax.ShapeDtypeStruct((seqs, pw), f32),
+            jax.ShapeDtypeStruct((n_ep, seqs, cols), bf16),
+            jax.ShapeDtypeStruct((n_ep, seqs, LANES), f32),
+        ),
+        in_specs=[vmem] * 7,
+        out_specs=(vmem,) * 3,
+        scratch_shapes=[
+            pltpu.VMEM((seqs, LANES), f32),
+            pltpu.VMEM((n_ep, seqs, pw), f32),
+            pltpu.VMEM((n_ep, seqs, pw), f32),
+        ]
+        + [dma((n_ep,))] * 6,
+        compiler_params=pltpu.CompilerParams(collective_id=0, has_side_effects=True),
+        name="front",
+    )(
+        tokens,
+        norm_gain.reshape(n_ep, cols),
+        wmat,
+        query_weight,
+        key_weight.T,
+        value_weight.T,
+        forget_weight.T,
+    )
+    queries = projected[:, :qc].astype(bf16)
+    key_new = projected[:, qc : qc + kc].astype(bf16)
+    value_new = projected[:, qc + kc : qc + 2 * kc].astype(bf16)
+    forget = jax.nn.log_sigmoid(projected[:, qc + 2 * kc : qc + 2 * kc + fc] + forget_bias)
+    attended = attend_local(queries, key_new, value_new, forget, kv_cache, log_gates, lengths)
+    cw = cols // n_tp
+    ocols = width // n_tp
+    return pl.pallas_call(
+        functools.partial(back_kernel, n_ep, n_tp),
+        out_shape=jax.ShapeDtypeStruct((seqs, ocols), bf16),
+        in_specs=[vmem] * 5 + [anywhere] * 7,
+        out_specs=vmem,
+        scratch_shapes=[
+            pltpu.VMEM(out_weight.shape, bf16),
+            pltpu.VMEM(expert_gate.shape[1:], bf16),
+            pltpu.VMEM(expert_up.shape[1:], bf16),
+            pltpu.VMEM(expert_down.shape[1:], bf16),
+            pltpu.VMEM(dense_gate.shape, bf16),
+            pltpu.VMEM(dense_up.shape, bf16),
+            pltpu.VMEM(dense_down.shape, bf16),
+            pltpu.VMEM((n_ep, seqs, attended.shape[1]), bf16),
+            pltpu.VMEM((n_tp, rows, cw), f32),
+            pltpu.VMEM((n_tp, rows, cw), f32),
+            pltpu.VMEM((n_tp, n_ep, rows, cw), bf16),
+            pltpu.VMEM((rows, width), bf16),
+            pltpu.VMEM((2, rows, ocols), f32),
+            pltpu.VMEM((2, rows, ocols), f32),
+            pltpu.VMEM((rows, ocols), bf16),
+            pltpu.VMEM((rows, ocols), bf16),
+            pltpu.VMEM((n_ep, seqs, ocols), bf16),
+            pltpu.VMEM((n_ep, seqs, ocols), bf16),
+            dma((7,)),
+            dma((2, n_ep)),
+            dma((2, n_tp)),
+            dma((2, n_ep)),
+            dma((2, n_ep)),
+            dma((2, 2, n_ep)),
+            dma((2, 2)),
+            dma((2,)),
+            dma((2, n_ep)),
+        ],
+        compiler_params=pltpu.CompilerParams(
+            collective_id=1, has_side_effects=True, vmem_limit_bytes=56 * 1024 * 1024
+        ),
+        name="back",
+    )(
+        attended,
+        token_cols,
+        aux,
+        mix_gain.reshape(1, width),
+        gate_vector.reshape(1, width),
+        out_weight,
+        expert_gate,
+        expert_up,
+        expert_down,
+        dense_gate,
+        dense_up,
+        dense_down,
+    )
+
+
+def layer(*arrays):
+    tokens, routes = arrays[0], arrays[15]
+    n_ep, n_tp = lax.axis_size("ep"), lax.axis_size("tp")
+    seqs, width = tokens.shape
+    capacity = seqs * routes.shape[1]
+    fits = (
+        n_tp == 4
+        and n_ep % n_tp == 0
+        and n_ep < LANES
+        and n_ep * seqs <= 2 * capacity
+        and width % (n_ep * n_tp * LANES) == 0
+        and arrays[2].shape[1] % LANES == 0
+    )
+    return (fused_shards if fits else shards)(*arrays)
+
+
 def solution(mesh):
     return jax.shard_map(
-        shards,
+        layer,
         mesh=mesh,
         in_specs=(
             P("ep", None),

time: 334 us -> 85.2 us (0.26)
  waiting for transfers between devices: 221 us -> 0 us
  Pallas kernels: 0 us -> 70 us
  blocking collectives: 44.9 us -> 0 us
  matrix products: 26.6 us -> 5.28 us
  starting transfers between devices: 14.8 us -> 0 us
  between operations: 13.5 us -> 0.06 us
  other arithmetic: 10.4 us -> 5.9 us
    reduce_scatter x3 -> x0, waiting for transfers between devices: 132 us -> none  [the longest x1 59.1 us: shards(): lax.psum_scatter(jnp.concatenate([jnp.dot(row_block, matrix, preferred_el...]
    pallas_call x0 -> x2, Pallas kernels: none -> 70 us  [the longest x1 49.5 us: fused_shards(): pl.pallas_call(functools.partial(back_kernel, n_ep, n_tp), out_shape=jax....]
    all_to_all x3 -> x0, waiting for transfers between devices: 43.6 us -> none  [the longest x1 27.4 us: shards(): lax.all_to_all(outgoing, 'ep', split_axis=0, concat_axis=0, tiled=True)]
    psum x1 -> x0, waiting for transfers between devices: 31.3 us -> none  [shards(): column_total = lax.psum(column_terms, 'tp')]
    all_gather x1 -> x0, blocking collectives: 30.5 us -> none  [shards(): lax.all_gather(attended, 'ep', axis=0, tiled=True)]
    dot_general x11 -> x0, matrix products: 21.3 us -> none  [the longest x1 4.29 us: shards(): jnp.dot(row_block, dense_down, preferred_element_type=jnp.float32)]
    all_to_all x3 -> x0, starting transfers between devices: 14.6 us -> none  [the longest x1 5.52 us: shards(): lax.all_to_all(replies, 'ep', split_axis=0, concat_axis=0, tiled=True)]
    all_to_all x1 -> x0, blocking collectives: 14.4 us -> none  [shards(): lax.all_to_all(normed, 'ep', split_axis=1, concat_axis=0, tiled=True)]
  transfers between devices with their start and end apart: 8 -> 0, of which waited for: 8 -> 0; matrix products, arithmetic and copies ran while one was open for 6% -> 0% of each run, Pallas kernels for 0% -> 0%
where the time goes in v1:
time: 85.2 us; the launch traced here: 84.8 us
  Pallas kernels  70 us (82%)
  other arithmetic  5.9 us (7%)
  matrix products  5.28 us (6%)
  local copies, waits for them, and re-layouts  3.51 us (4%)
    pallas_call x1, Pallas kernels, fused_shards(): pl.pallas_call(functools.partial(back_kernel, n_ep, n_tp), out_shape=jax....  49.5 us
    pallas_call x1, Pallas kernels, fused_shards(): pl.pallas_call(functools.partial(front_kernel, n_ep), out_shape=(jax.Shap...  20.5 us
    dot_general x1, matrix products, attend_local(): jnp.einsum('skgd,slkd->skgl', queries, cached_keys, preferred_element_typ...  3.74 us

profile of v1, /device:TPU:0, one launch (start us, length us, event | category | flops | bytes accessed | tf_op | source)
XLA Modules:
  0.0 84.8 jit_solution(13682399561351140995)
XLA Ops:
  0.0 0.7 broadcast_add_fusion
  0.7 1.4 %select_reduce_fusion.1.wmat_ref = f32[16,128]{1,0:T(8,128)} fusion(f32[16,4]{0,1:T(4,128)} %param.37, s32[16,4]{0,1:T(4,128)} %param.36), kind=kLoop, calls=%fused_computation.20 | loop fusion | flops 22528 | bytes 8704 | tf_op jit(solution)/shard_map/reduce_sum | solution.py:505
  2.0 0.1 iota_compare_fusion
  2.1 1.2 %select_reduce_fusion = f32[16,8]{1,0:T(8,128)S(1)} fusion(f32[16,1024,8]{1,2,0:T(8,128)} %param.29, pred[16,1024]{1,0:T(8,128)(4,1)S(1)} %iota_compare_fusion), kind=kLoop, calls=%fused_computation.14 | loop fusion | flops 262016 | bytes 541184 | tf_op jit(solution)/shard_map/reduce_sum | solution.py:30
  3.3 1.3 %reshape.119.gain_ref = f32[8,512]{1,0:T(8,128)} reshape(f32[4096]{0:T(1024)} %param.22) | data formatting | bytes 32768 | tf_op jit(solution)/shard_map/reshape | solution.py:525
  4.6 0.7 iota_compare_fusion.1
  5.4 20.5 %front.1 = (f32[16,768]{1,0:T(8,128)}, bf16[8,16,512]{2,1,0:T(8,128)(2,1)}, f32[8,16,128]{2,1,0:T(8,128)}) custom-call(bf16[16,4096]{1,0:T(8,128)(2,1)} %tok_ref.1, f32[8,512]{1,0:T(8,128)} %reshape.119.gain_ref, f32[16,128]{1,0:T(8,128)} %select_reduce_fusion.1.wmat_ref, bf16[512,512]{1,0:T(8,128)(2,1)} %wq_ref.1, bf16[64,512]{1,0:T(8,128)(2,1)} %bitcast.46, ...), custom_call_target="tpu_custom_call" | custom-call | tf_op jit(solution)/shard_map/front/pallas_call | solution.py:506
  25.9 0.7 fusion.28
  26.6 0.8 convert.5
  27.4 0.1 slice_convert_fusion
  27.5 0.1 reshape.120
  27.6 0.0 copy-start
  27.6 0.1 fusion.29
  27.8 3.7 %fusion.33 = (f32[16,8]{1,0:T(8,128)S(1)}, f32[16,1,8,1024]{3,2,0,1:T(8,128)S(1)}) fusion(f32[16,1024,8]{1,2,0:T(8,128)} %param.29, f32[16,8]{1,0:T(8,128)S(1)} %fusion.28, bf16[16,8,64]{2,1,0:T(8,128)(2,1)S(1)} %reshape.120, bf16[16,1024,1,128]{3,1,2,0:T(8,128)(2,1)} %param.28, pred[16,1024]{1,0:T(8,128)(4,1)S(1)} %iota_compare_fusion.1), kind=kOutput, calls=%fused_computation.35 | convolution fusion | flops 17432448 | bytes 5276672 | tf_op jit(solution)/shard_map/skgd,slkd->skgl/dot_general | solution.py:35
  31.5 0.2 fusion.24
  31.8 0.0 copy-done
  31.8 1.4 %fusion.21 = bf16[16,8,64]{2,1,0:T(8,128)(2,1)S(1)} fusion(bf16[16,1024,1,128]{3,1,2,0:T(8,128)(2,1)S(1)} %copy-done, f32[16,1,8,1024]{3,2,0,1:T(8,128)S(1)} %get-tuple-element.16, f32[16,8]{1,0:T(8,128)S(1)} %get-tuple-element.12, f32[16,8]{1,0:T(8,128)S(1)} %multiply_maximum_fusion, f32[16,64]{1,0:T(8,128)S(1)} %get-tuple-element.13, ...), kind=kOutput, calls=%fused_computation.11 | convolution fusion | flops 17195008 | bytes 4740608 | tf_op jit(solution)/shard_map/skgl,slkd->skgd/dot_general | solution.py:51
  33.2 0.7 reshape.125.att_ref
  33.9 49.5 %back.1 = bf16[16,1024]{1,0:T(8,128)(2,1)} custom-call(bf16[16,512]{1,0:T(8,128)(2,1)} %reshape.125.att_ref, bf16[8,16,512]{2,1,0:T(8,128)(2,1)} %get-tuple-element.9.tokc_ref, f32[8,16,128]{2,1,0:T(8,128)} %get-tuple-element.10.aux_ref, f32[1,4096]{1,0:T(1,128)} %bitcast.50, f32[1,4096]{1,0:T(1,128)} %bitcast.51, bf16[512,512]{1,0:T(8,128)(2,1)} %ow_hbm.1, ...), custom_call_target="tpu_custom_call" | custom-call | tf_op jit(solution)/shard_map/back/pallas_call | solution.py:539
  83.4 1.4 %copy.35 = bf16[16,1024]{1,0:T(8,128)(2,1)} copy(bf16[16,1024]{1,0:T(8,128)(2,1)} %back.1) | data formatting | bytes 65536
  (3 shorter events, 0.0 us)
Async XLA Ops:
  27.6 4.1 %copy-start = (bf16[16,1024,1,128]{3,1,2,0:T(8,128)(2,1)S(1)}, bf16[16,1024,1,128]{3,1,2,0:T(8,128)(2,1)}, u32[]{:S(2)}) copy-start(bf16[16,1024,1,128]{3,1,2,0:T(8,128)(2,1)} %param.28) | copy-start | bytes 12582916

commit v2 on v1

--- a/solution.py
+++ b/solution.py
@@ -190,88 +190,23 @@
     return copy
 
 
-def front_kernel(
+def layer_kernel(
     n_ep,
+    n_tp,
     tok_ref,
     gain_ref,
-    wmat_ref,
-    wq_ref,
+    routes_ref,
+    weights_ref,
     wk_ref,
     wv_ref,
     wf_ref,
-    proj_ref,
-    tokc_ref,
-    aux_ref,
-    aux_own,
-    part,
-    part_in,
-    ts_sem,
-    tr_sem,
-    as_sem,
-    ar_sem,
-    ps_sem,
-    pr_sem,
-):
-    e = lax.axis_index("ep")
-    t = lax.axis_index("tp")
-    seqs, width = tok_ref.shape
-    cols = width // n_ep
-    barrier = pltpu.get_barrier_semaphore()
-    for o in range(1, n_ep):
-        pl.semaphore_signal(
-            barrier, inc=1, device_id=(lax.rem(e + o, n_ep), t), device_id_type=MESH
-        )
-    tokens = tok_ref[...].astype(jnp.float32)
-    scale = lax.rsqrt(jnp.mean(tokens * tokens, axis=-1, keepdims=True) + EPS)
-    lane = lax.broadcasted_iota(jnp.int32, (seqs, LANES), 1)
-    aux_own[...] = jnp.where(lane == LANES - 1, scale, wmat_ref[...])
-    pl.semaphore_wait(barrier, n_ep - 1)
-    copies = []
-    for o in range(1, n_ep):
-        peer = lax.rem(e + o, n_ep)
-        chunk = pl.ds(pl.multiple_of(peer * cols, LANES), cols)
-        copies.append(
-            remote(tok_ref.at[:, chunk], tokc_ref.at[e], ts_sem.at[o], tr_sem.at[o], peer, t)
-        )
-        copies.append(remote(aux_own, aux_ref.at[e], as_sem.at[o], ar_sem.at[o], peer, t))
-    tokc_ref[e] = tok_ref[:, pl.ds(pl.multiple_of(e * cols, LANES), cols)]
-    aux_ref[e] = aux_own[...]
-    for copy in copies:
-        copy.wait_recv()
-    rows = n_ep * seqs
-    scales = aux_ref[...].reshape(rows, LANES)[:, LANES - 1 :]
-    block = tokc_ref[...].reshape(rows, cols).astype(jnp.float32)
-    normed = (block * scales * gain_ref[pl.ds(e, 1), :]).astype(jnp.bfloat16)
-    queries = jnp.dot(normed, wq_ref[...], preferred_element_type=jnp.float32)
-    qc = queries.shape[1]
-    kc = wk_ref.shape[0]
-    fc = wf_ref.shape[0]
-    part[:, :, :qc] = queries.reshape(n_ep, seqs, qc)
-    rest = [nt_dot(normed, wk_ref[...]), nt_dot(normed, wv_ref[...]), nt_dot(normed, wf_ref[...])]
-    fill = part.shape[2] - qc - 2 * kc - fc
-    rest = jnp.concatenate(rest + [jnp.zeros((rows, fill), jnp.float32)], axis=1)
-    part[:, :, qc:] = rest.reshape(n_ep, seqs, rest.shape[1])
-    sums = []
-    for o in range(1, n_ep):
-        peer = lax.rem(e + o, n_ep)
-        sums.append(remote(part.at[peer], part_in.at[o], ps_sem.at[o], pr_sem.at[o], peer, t))
-    total = part[e]
-    for o in range(1, n_ep):
-        sums[o - 1].wait_recv()
-        total = total + part_in[o]
-    proj_ref[...] = total
-    for copy in copies + sums:
-        copy.wait_send()
-
-
-def back_kernel(
-    n_ep,
-    n_tp,
-    att_ref,
-    tokc_ref,
-    aux_ref,
-    gain_ref,
+    bias_ref,
+    mgain_ref,
     vector_ref,
+    lengths_ref,
+    wq_hbm,
+    kv_hbm,
+    gates_hbm,
     ow_hbm,
     eg_hbm,
     eu_hbm,
@@ -280,6 +215,20 @@
     du_hbm,
     dd_hbm,
     out_ref,
+    tokc,
+    aux_own,
+    aux_all,
+    part,
+    part_in,
+    wq,
+    kv,
+    lgates,
+    qs,
+    score,
+    prob,
+    heads,
+    att_own,
+    att,
     ow,
     eg,
     eu,
@@ -287,89 +236,190 @@
     dg,
     du,
     dd,
-    att,
     osend,
     orecv,
     mix,
     sec,
-    dsend,
-    drecv,
-    ysend,
-    yrecv,
+    hid,
     csend,
     crecv,
     w_sem,
+    e_sem,
+    t_sem,
+    x_sem,
+    p_sem,
     a_sem,
     o_sem,
     g_sem,
     gy_sem,
     gd_sem,
-    d_sem,
-    y_sem,
+    h_sem,
     c_sem,
 ):
     e = lax.axis_index("ep")
     t = lax.axis_index("tp")
     ty = lax.rem(t + 2, n_tp)
     td = t + 1 - 2 * lax.rem(t, 2)
-    tdy = lax.rem(td + 2, n_tp)
-    seqs = att_ref.shape[0]
+    seqs, width = tok_ref.shape
     rows = n_ep * seqs
+    cols = width // n_ep
+    ocols = width // n_tp
+    bf16, f32 = jnp.bfloat16, jnp.float32
+    barrier = pltpu.get_barrier_semaphore()
+    for o in range(1, n_ep):
+        pl.semaphore_signal(
+            barrier, inc=1, device_id=(lax.rem(e + o, n_ep), t), device_id_type=MESH
+        )
+    for o in range(1, n_tp):
+        pl.semaphore_signal(
+            barrier, inc=1, device_id=(e, lax.rem(t + o, n_tp)), device_id_type=MESH
+        )
+    own_cols = pl.ds(pl.multiple_of(t * ocols, LANES), ocols)
     loads = [
         pltpu.make_async_copy(src, dst, w_sem.at[i])
         for i, (src, dst) in enumerate(
             [
+                (wq_hbm, wq),
+                (gates_hbm, lgates),
+                (kv_hbm, kv),
                 (ow_hbm, ow),
                 (eg_hbm.at[0], eg),
                 (eu_hbm.at[0], eu),
-                (ed_hbm.at[0], ed),
                 (dg_hbm, dg),
                 (du_hbm, du),
                 (dd_hbm, dd),
+                (ed_hbm.at[0, :, own_cols], ed.at[t]),
             ]
         )
     ]
     for load in loads:
         load.start()
-    barrier = pltpu.get_barrier_semaphore()
-    for o in range(1, n_ep):
-        pl.semaphore_signal(
-            barrier, inc=1, device_id=(lax.rem(e + o, n_ep), t), device_id_type=MESH
-        )
-    for o in range(1, n_tp):
-        pl.semaphore_signal(
-            barrier, inc=1, device_id=(e, lax.rem(t + o, n_tp)), device_id_type=MESH
-        )
+    tokens = tok_ref[...].astype(f32)
+    scale = lax.rsqrt(jnp.mean(tokens * tokens, axis=-1, keepdims=True) + EPS)
+    lane = lax.broadcasted_iota(jnp.int32, (seqs, LANES), 1)
+    lane_f = lane.astype(f32)
+    eye = lax.broadcasted_iota(jnp.int32, (seqs, seqs), 0) == lax.broadcasted_iota(
+        jnp.int32, (seqs, seqs), 1
+    )
+    table = jnp.where(lane == LANES - 1, scale, 0.0)
+    for k in range(routes_ref.shape[0]):
+        picked = routes_ref[k : k + 1, :].astype(f32)
+        picked = jnp.sum(jnp.where(eye, picked, 0.0), axis=-1, keepdims=True)
+        amount = jnp.sum(jnp.where(eye, weights_ref[k : k + 1, :], 0.0), axis=-1, keepdims=True)
+        table = table + jnp.where(lane_f == picked, amount, 0.0)
+    aux_own[...] = table
     pl.semaphore_wait(barrier, n_ep + n_tp - 2)
     pending = []
     copies = []
     for o in range(1, n_ep):
         peer = lax.rem(e + o, n_ep)
-        copies.append(remote(att_ref, att.at[e], a_sem.at[0, o], a_sem.at[1, o], peer, t))
-    att[e] = att_ref[...]
-    loads[0].wait()
+        chunk = pl.ds(pl.multiple_of(peer * cols, LANES), cols)
+        copies.append(
+            remote(tok_ref.at[:, chunk], tokc.at[e], t_sem.at[0, o], t_sem.at[1, o], peer, t)
+        )
+        copies.append(remote(aux_own, aux_all.at[e], x_sem.at[0, o], x_sem.at[1, o], peer, t))
+    down_copies = []
+    for o in range(1, n_tp):
+        peer = lax.rem(t + o, n_tp)
+        chunk = pl.ds(pl.multiple_of(peer * ocols, LANES), ocols)
+        down_copies.append(
+            remote(
+                ed_hbm.at[0, :, chunk], ed.at[t], e_sem.at[0, o], e_sem.at[1, o], e, peer
+            )
+        )
+    tokc[e] = tok_ref[:, pl.ds(pl.multiple_of(e * cols, LANES), cols)]
+    aux_all[e] = aux_own[...]
     for copy in copies:
         copy.wait_recv()
     pending += copies
-    partial = jnp.dot(
-        att[...].reshape(rows, att_ref.shape[1]), ow[...], preferred_element_type=jnp.float32
-    )
-    cw = osend.shape[2]
-    for j in range(n_tp):
-        osend[j] = partial[:, j * cw : (j + 1) * cw]
+    aux = aux_all[...].reshape(rows, LANES)
+    block = tokc[...].reshape(rows, cols).astype(f32)
+    gain = gain_ref[:, pl.ds(pl.multiple_of(e * cols, LANES), cols)]
+    normed = (block * aux[:, LANES - 1 :] * gain).astype(bf16)
+    loads[0].wait()
+    queries = jnp.dot(normed, wq[...], preferred_element_type=f32)
+    qc = queries.shape[1]
+    hd = wk_ref.shape[0]
+    group = wf_ref.shape[0]
+    part[:, :, :qc] = queries.reshape(n_ep, seqs, qc)
+    rest = [nt_dot(normed, wk_ref[...]), nt_dot(normed, wv_ref[...]), nt_dot(normed, wf_ref[...])]
+    fill = part.shape[2] - qc - 2 * hd - group
+    rest = jnp.concatenate(rest + [jnp.zeros((rows, fill), f32)], axis=1)
+    part[:, :, qc:] = rest.reshape(n_ep, seqs, rest.shape[1])
+    sums = []
+    for o in range(1, n_ep):
+        peer = lax.rem(e + o, n_ep)
+        sums.append(remote(part.at[peer], part_in.at[o], p_sem.at[0, o], p_sem.at[1, o], peer, t))
+    total = part[e]
+    for o in range(1, n_ep):
+        sums[o - 1].wait_recv()
+        total = total + part_in[o]
+    pending += sums
+    rounded = total[:, : qc + 2 * hd].astype(bf16).astype(f32)
+    fresh = rounded[:, qc:]
+    forget = jax.nn.log_sigmoid(total[:, qc + 2 * hd : qc + 2 * hd + group] + bias_ref[...])
+    zeros = jnp.zeros((seqs, hd), f32)
+    for g in range(group):
+        qs[:, g, :] = jnp.concatenate([rounded[:, g * hd : (g + 1) * hd], zeros], axis=1)
+    loads[1].wait()
+    loads[2].wait()
+    for s in range(seqs):
+        score[s] = nt_dot(qs[s].astype(bf16), kv[s])
+    inverse = hd ** (-0.5)
+    count = kv.shape[1]
+    place = lax.broadcasted_iota(jnp.int32, (group, count), 1)
+    square = lax.broadcasted_iota(jnp.int32, (group, group), 0) == lax.broadcasted_iota(
+        jnp.int32, (group, group), 1
+    )
+    own_weights = []
+    for s in range(seqs):
+        length = lengths_ref[s]
+        levels = lgates[s]
+        last = jnp.sum(jnp.where(place == length - 1, levels, 0.0), axis=-1, keepdims=True)
+        newest = last + jnp.sum(
+            jnp.where(square, forget[s : s + 1, :], 0.0), axis=-1, keepdims=True
+        )
+        past = jnp.where(place < length, score[s] * inverse + (newest - levels), -jnp.inf)
+        own = jnp.sum(qs[s] * fresh[s : s + 1, :], axis=-1, keepdims=True) * inverse
+        highest = jnp.maximum(jnp.max(past, axis=-1, keepdims=True), own)
+        past = jnp.exp(past - highest)
+        own = jnp.exp(own - highest)
+        whole = jnp.sum(past, axis=-1, keepdims=True) + own
+        prob[s] = (past / whole).astype(bf16)
+        own_weights.append((own / whole).astype(bf16).astype(f32))
+    for s in range(seqs):
+        values = jnp.dot(prob[s], kv[s], preferred_element_type=f32)
+        heads[s] = values + own_weights[s] * fresh[s : s + 1, :]
+    att_own[...] = jnp.concatenate([heads[:, g, hd:] for g in range(group)], axis=1).astype(bf16)
     copies = []
+    for o in range(1, n_ep):
+        peer = lax.rem(e + o, n_ep)
+        copies.append(remote(att_own, att.at[e], a_sem.at[0, o], a_sem.at[1, o], peer, t))
+    att[e] = att_own[...]
+    loads[3].wait()
+    for copy in copies:
+        copy.wait_recv()
+    pending += copies
+    gathered = att[...].reshape(rows, att.shape[2])
+    cw = cols // n_tp
+
+    def out_columns(owner):
+        chunk = pl.ds(pl.multiple_of(owner * cw, LANES), cw)
+        return jnp.dot(gathered, ow[:, chunk], preferred_element_type=f32)
+
+    copies = []
+    for o in (2, 1, 3):
+        peer = lax.rem(t + o, n_tp)
+        osend[o] = out_columns(peer).astype(bf16)
+        copies.append(remote(osend.at[o], orecv.at[o], o_sem.at[0, o], o_sem.at[1, o], e, peer))
+    total = out_columns(t)
+    for copy in copies:
+        copy.wait_recv()
     for o in range(1, n_tp):
-        peer = lax.rem(t + o, n_tp)
-        copies.append(
-            remote(osend.at[peer], orecv.at[o], o_sem.at[0, o], o_sem.at[1, o], e, peer)
-        )
-    total = osend[t]
-    for o in range(1, n_tp):
-        copies[o - 1].wait_recv()
-        total = total + orecv[o]
+        total = total + orecv[o].astype(f32)
     pending += copies
-    own_tokens = tokc_ref[:, :, pl.ds(pl.multiple_of(t * cw, LANES), cw)].reshape(rows, cw)
-    mix[t, e] = (own_tokens.astype(jnp.float32) + total).astype(jnp.bfloat16)
+    own_tokens = tokc[:, :, pl.ds(pl.multiple_of(t * cw, LANES), cw)].reshape(rows, cw)
+    mix[t, e] = (own_tokens.astype(f32) + total).astype(bf16)
     arrivals, y_copies, d_copies = [], [], []
     for o in range(1, n_ep):
         peer = lax.rem(e + o, n_ep)
@@ -402,46 +452,37 @@
     for i in range(n_ep):
         for j in range(n_tp):
             at = (i * n_tp + j) * cw
-            values = mix[j, i].astype(jnp.float32) * scale * gain_ref[:, at : at + cw]
+            values = mix[j, i].astype(jnp.float32) * scale * mgain_ref[:, at : at + cw]
             values = values.astype(jnp.bfloat16)
             sec[:, at : at + cw] = values
             gates = gates + values.astype(jnp.float32) * vector_ref[:, at : at + cw]
     gate_value = jax.nn.sigmoid(jnp.sum(gates, axis=-1, keepdims=True))
-    for load in loads[1:4]:
+    for load in loads[4:6]:
         load.wait()
-    hidden = (
-        jax.nn.silu(jnp.dot(sec[...], eg[...], preferred_element_type=jnp.float32))
-        * jnp.dot(sec[...], eu[...], preferred_element_type=jnp.float32)
-    ).astype(jnp.bfloat16)
-    ocols = out_ref.shape[1]
-
-    def down(owner):
-        chunk = pl.ds(pl.multiple_of(owner * ocols, LANES), ocols)
-        return jnp.dot(hidden, ed[:, chunk], preferred_element_type=jnp.float32)
-
-    pair = []
-    for k, owner in enumerate((tdy, td)):
-        dsend[k] = down(owner)
-        pair.append(
-            remote(dsend.at[k], drecv.at[k], d_sem.at[0, k], d_sem.at[1, k], e, td)
-        )
-    across = down(ty)
-    pair[0].wait_recv()
-    ysend[...] = (across + drecv[0]).astype(jnp.bfloat16)
-    y_copy = remote(ysend, yrecv, y_sem.at[0], y_sem.at[1], e, ty)
-    own = down(t)
-    for load in loads[4:]:
+    hid[t] = (
+        jax.nn.silu(jnp.dot(sec[...], eg[...], preferred_element_type=f32))
+        * jnp.dot(sec[...], eu[...], preferred_element_type=f32)
+    ).astype(bf16)
+    hidden_copies = []
+    for o in (2, 1, 3):
+        peer = lax.rem(t + o, n_tp)
+        hidden_copies.append(
+            remote(hid.at[t], hid.at[t], h_sem.at[0, o], h_sem.at[1, o], e, peer)
+        )
+    for load in loads[6:]:
         load.wait()
     dense_hidden = (
-        jax.nn.silu(jnp.dot(sec[...], dg[...], preferred_element_type=jnp.float32))
-        * jnp.dot(sec[...], du[...], preferred_element_type=jnp.float32)
-    ).astype(jnp.bfloat16)
-    dense = jnp.dot(dense_hidden, dd[...], preferred_element_type=jnp.float32)
-    pair[1].wait_recv()
-    y_copy.wait_recv()
-    expert_out = (own + drecv[1] + yrecv[...].astype(jnp.float32)).astype(jnp.bfloat16)
-    pending += pair + [y_copy]
-    aux = aux_ref[...].reshape(rows, LANES)
+        jax.nn.silu(jnp.dot(sec[...], dg[...], preferred_element_type=f32))
+        * jnp.dot(sec[...], du[...], preferred_element_type=f32)
+    ).astype(bf16)
+    dense = jnp.dot(dense_hidden, dd[...], preferred_element_type=f32)
+    for copy in down_copies + hidden_copies:
+        copy.wait_recv()
+    pending += down_copies + hidden_copies
+    expert_out = jnp.dot(hid[0], ed[0], preferred_element_type=f32)
+    for j in range(1, n_tp):
+        expert_out = expert_out + jnp.dot(hid[j], ed[j], preferred_element_type=f32)
+    expert_out = expert_out.astype(bf16)
     lane = lax.broadcasted_iota(jnp.int32, (rows, LANES), 1)
     weight = jnp.sum(jnp.where(lane == e, aux, 0.0), axis=-1, keepdims=True)
     terms = weight * expert_out.astype(jnp.float32) + gate_value * dense
@@ -493,93 +534,84 @@
     seqs, width = tokens.shape
     rows = n_ep * seqs
     cols = width // n_ep
+    cw = cols // n_tp
+    ocols = width // n_tp
     qc = query_weight.shape[1]
-    kc = key_weight.shape[1]
-    fc = forget_weight.shape[1]
-    pw = qc + -(-(2 * kc + fc) // LANES) * LANES
+    hd = key_weight.shape[1]
+    group = forget_weight.shape[1]
+    count = kv_cache.shape[1]
+    pw = qc + -(-(2 * hd + group) // LANES) * LANES
     vmem = pl.BlockSpec(memory_space=pltpu.VMEM)
+    smem = pl.BlockSpec(memory_space=pltpu.SMEM)
     anywhere = pl.BlockSpec(memory_space=pl.ANY)
     dma = pltpu.SemaphoreType.DMA
     f32, bf16 = jnp.float32, jnp.bfloat16
-    chosen = routes[:, :, None] == jnp.arange(LANES, dtype=jnp.int32)[None, None, :]
-    wmat = jnp.sum(jnp.where(chosen, route_weights[:, :, None], 0.0), axis=1)
-    projected, token_cols, aux = pl.pallas_call(
-        functools.partial(front_kernel, n_ep),
-        out_shape=(
-            jax.ShapeDtypeStruct((seqs, pw), f32),
-            jax.ShapeDtypeStruct((n_ep, seqs, cols), bf16),
-            jax.ShapeDtypeStruct((n_ep, seqs, LANES), f32),
-        ),
-        in_specs=[vmem] * 7,
-        out_specs=(vmem,) * 3,
+    return pl.pallas_call(
+        functools.partial(layer_kernel, n_ep, n_tp),
+        out_shape=jax.ShapeDtypeStruct((seqs, ocols), bf16),
+        in_specs=[vmem] * 10 + [smem] + [anywhere] * 10,
+        out_specs=vmem,
         scratch_shapes=[
+            pltpu.VMEM((n_ep, seqs, cols), bf16),
             pltpu.VMEM((seqs, LANES), f32),
+            pltpu.VMEM((n_ep, seqs, LANES), f32),
             pltpu.VMEM((n_ep, seqs, pw), f32),
             pltpu.VMEM((n_ep, seqs, pw), f32),
-        ]
-        + [dma((n_ep,))] * 6,
-        compiler_params=pltpu.CompilerParams(collective_id=0, has_side_effects=True),
-        name="front",
-    )(
-        tokens,
-        norm_gain.reshape(n_ep, cols),
-        wmat,
-        query_weight,
-        key_weight.T,
-        value_weight.T,
-        forget_weight.T,
-    )
-    queries = projected[:, :qc].astype(bf16)
-    key_new = projected[:, qc : qc + kc].astype(bf16)
-    value_new = projected[:, qc + kc : qc + 2 * kc].astype(bf16)
-    forget = jax.nn.log_sigmoid(projected[:, qc + 2 * kc : qc + 2 * kc + fc] + forget_bias)
-    attended = attend_local(queries, key_new, value_new, forget, kv_cache, log_gates, lengths)
-    cw = cols // n_tp
-    ocols = width // n_tp
-    return pl.pallas_call(
-        functools.partial(back_kernel, n_ep, n_tp),
-        out_shape=jax.ShapeDtypeStruct((seqs, ocols), bf16),
-        in_specs=[vmem] * 5 + [anywhere] * 7,
-        out_specs=vmem,
-        scratch_shapes=[
+            pltpu.VMEM(query_weight.shape, bf16),
+            pltpu.VMEM((seqs, count, 2 * hd), bf16),
+            pltpu.VMEM((seqs, group, count), f32),
+            pltpu.VMEM((seqs, group, 2 * hd), f32),
+            pltpu.VMEM((seqs, group, count), f32),
+            pltpu.VMEM((seqs, group, count), bf16),
+            pltpu.VMEM((seqs, group, 2 * hd), f32),
+            pltpu.VMEM((seqs, qc), bf16),
+            pltpu.VMEM((n_ep, seqs, qc), bf16),
             pltpu.VMEM(out_weight.shape, bf16),
             pltpu.VMEM(expert_gate.shape[1:], bf16),
             pltpu.VMEM(expert_up.shape[1:], bf16),
-            pltpu.VMEM(expert_down.shape[1:], bf16),
+            pltpu.VMEM((n_tp, expert_down.shape[1], ocols), bf16),
             pltpu.VMEM(dense_gate.shape, bf16),
             pltpu.VMEM(dense_up.shape, bf16),
             pltpu.VMEM(dense_down.shape, bf16),
-            pltpu.VMEM((n_ep, seqs, attended.shape[1]), bf16),
-            pltpu.VMEM((n_tp, rows, cw), f32),
-            pltpu.VMEM((n_tp, rows, cw), f32),
+            pltpu.VMEM((n_tp, rows, cw), bf16),
+            pltpu.VMEM((n_tp, rows, cw), bf16),
             pltpu.VMEM((n_tp, n_ep, rows, cw), bf16),
             pltpu.VMEM((rows, width), bf16),
-            pltpu.VMEM((2, rows, ocols), f32),
-            pltpu.VMEM((2, rows, ocols), f32),
-            pltpu.VMEM((rows, ocols), bf16),
-            pltpu.VMEM((rows, ocols), bf16),
+            pltpu.VMEM((n_tp, rows, expert_gate.shape[2]), bf16),
             pltpu.VMEM((n_ep, seqs, ocols), bf16),
             pltpu.VMEM((n_ep, seqs, ocols), bf16),
-            dma((7,)),
+            dma((10,)),
+            dma((2, n_tp)),
+            dma((2, n_ep)),
+            dma((2, n_ep)),
+            dma((2, n_ep)),
             dma((2, n_ep)),
             dma((2, n_tp)),
             dma((2, n_ep)),
             dma((2, n_ep)),
             dma((2, 2, n_ep)),
-            dma((2, 2)),
-            dma((2,)),
+            dma((2, n_tp)),
             dma((2, n_ep)),
         ],
         compiler_params=pltpu.CompilerParams(
-            collective_id=1, has_side_effects=True, vmem_limit_bytes=56 * 1024 * 1024
+            collective_id=0, has_side_effects=True, vmem_limit_bytes=56 * 1024 * 1024
         ),
-        name="back",
+        name="layer",
     )(
-        attended,
-        token_cols,
-        aux,
+        tokens,
+        norm_gain.reshape(1, width),
+        routes.T,
+        route_weights.T,
+        key_weight.T,
+        value_weight.T,
+        forget_weight.T,
+        forget_bias.reshape(1, group),
         mix_gain.reshape(1, width),
         gate_vector.reshape(1, width),
+        lengths,
+        query_weight,
+        kv_cache.reshape(seqs, count, 2 * hd),
+        log_gates.transpose(0, 2, 1),
         out_weight,
         expert_gate,
         expert_up,
@@ -602,6 +634,8 @@
         and n_ep * seqs <= 2 * capacity
         and width % (n_ep * n_tp * LANES) == 0
         and arrays[2].shape[1] % LANES == 0
+        and arrays[7].shape[2] == 1
+        and arrays[7].shape[3] == LANES
     )
     return (fused_shards if fits else shards)(*arrays)
 

time: 85.2 us -> 65.8 us (0.77)
  other arithmetic: 5.9 us -> 0 us
  Pallas kernels: 70 us -> 64.2 us
  matrix products: 5.28 us -> 0 us
  local copies, waits for them, and re-layouts: 3.51 us -> 1.38 us
    pallas_call x2 -> x1, Pallas kernels: 70 us -> 64.2 us  [fused_shards(): pl.pallas_call(functools.partial(layer_kernel, n_ep, n_tp), out_shape=jax...]
    dot_general x3 -> x0, matrix products: 5.28 us -> none  [the longest x1 3.74 us: attend_local(): jnp.einsum('skgd,slkd->skgl', queries, cached_keys, preferred_element_typ...]
    reduce_sum x3 -> x0, other arithmetic: 2.82 us -> none  [the longest x1 1.37 us: fused_shards(): wmat = jnp.sum(jnp.where(chosen, route_weights[:, :, None], 0.0), axis=1)]
    reshape x2 -> x0, local copies, waits for them, and re-layouts: 2.03 us -> none  [the longest x1 1.32 us: fused_shards(): norm_gain.reshape(n_ep, cols)]
where the time goes in v2:
time: 65.8 us; the launch traced here: 65.6 us
  Pallas kernels  64.2 us (98%)
  local copies, waits for them, and re-layouts  1.38 us (2%)
    pallas_call x1, Pallas kernels, fused_shards(): pl.pallas_call(functools.partial(layer_kernel, n_ep, n_tp), out_shape=jax...  64.2 us
    unnamed x1, local copies, waits for them, and re-layouts  1.38 us

profile of v2, /device:TPU:0, one launch (start us, length us, event | category | flops | bytes accessed | tf_op | source)
XLA Modules:
  0.0 65.6 jit_solution(13433671913859178373)
XLA Ops:
  0.0 64.2 %layer.1 = bf16[16,1024]{1,0:T(8,128)(2,1)} custom-call(bf16[16,4096]{1,0:T(8,128)(2,1)} %tok_ref.1, f32[1,4096]{1,0:T(1,128)} %bitcast.15, s32[4,16]{1,0:T(4,128)} %bitcast.19, f32[4,16]{1,0:T(4,128)} %bitcast.20, bf16[64,512]{1,0:T(8,128)(2,1)} %bitcast.13, bf16[64,512]{1,0:T(8,128)(2,1)} %bitcast.14, bf16[8,512]{1,0:T(8,128)(2,1)} %bitcast.18, ...), custom_call_target="tpu_custom_call" | custom-call | tf_op jit(solution)/shard_map/layer/pallas_call | solution.py:549
  64.2 1.4 %copy.23 = bf16[16,1024]{1,0:T(8,128)(2,1)} copy(bf16[16,1024]{1,0:T(8,128)(2,1)} %layer.1) | data formatting | bytes 65536
